TPU v7x, 128 devices: a whole 4x4x4 slice. The times are simulated.
128 devices in a mesh: fs: 32 (over z, y, core), tp: 4 (over x).
Axes of the slice: x: 4, y: 4, z: 4, core: 2. Of those that a mesh axis runs over, the one named last changes fastest.
Arguments:
- normed_input: bfloat16 [147456, 2048], P('fs'), may hold values from -12 to 12
- query_latent_cotangent: bfloat16 [147456, 768], P('fs', 'tp'), may hold values from -0.015625 to 0.015625
- key_value_latent_cotangent: bfloat16 [147456, 512], P('fs', 'tp'), may hold values from -0.015625 to 0.015625
- row_factor: bfloat16 [2048, 256], P('fs'), may hold values from -0.25 to 0.25
- query_down_weight: float32 [2048, 768], P('fs', 'tp'), may hold values from -6 to 6
- key_value_down_weight: float32 [2048, 512], P('fs', 'tp'), may hold values from -6 to 6
- query_first_moment: float32 [256, 768], P('fs', 'tp'), may hold values from -6 to 6
- key_value_first_moment: float32 [256, 512], P('fs', 'tp'), may hold values from -6 to 6
- query_second: float32 [256, 768], P('fs', 'tp'), may hold values from 0.5 to 2000
- latent_second: float32 [256, 512], P('fs', 'tp'), may hold values from 0.5 to 2000
Outputs:
- query_new: float32 [2048, 768], P('fs', 'tp')
- latent_new: float32 [2048, 512], P('fs', 'tp')
- query_step: float32 [2048, 768], P('fs', 'tp')
- latent_step: float32 [2048, 512], P('fs', 'tp')
- query_copy: bfloat16 [2048, 768], P(None, 'tp')
- latent_copy: bfloat16 [2048, 512], P(None, 'tp')
- query_first_new: float32 [256, 768], P('fs', 'tp')
- latent_first_new: float32 [256, 512], P('fs', 'tp')
- query_second_new: float32 [256, 768], P('fs', 'tp')
- latent_second_new: float32 [256, 512], P('fs', 'tp')
All inputs are finite; a program needn't handle non-finite values.
Results may differ from a plain program's by a relative error of at most 0.006.
Values may be sent and summed in bfloat16 or wider, within the bound.
A program may use at most 64 MiB of HBM per device.

v0:
```python
import functools

import jax
import jax.numpy as jnp
from jax import lax
from jax.sharding import Mesh
from jax.sharding import PartitionSpec as P

FS = ("fs_0", "fs_1", "fs_2")
FS_TP = ("fs_0", "fs_1", "fs_2", "tp")


def from_everyone(array, axis):
    copies = jnp.broadcast_to(array, (lax.axis_size(axis), *array.shape))
    return lax.all_to_all(copies, axis, split_axis=0, concat_axis=0, tiled=True)


def in_order(tiles, dim):
    tiles = jnp.moveaxis(tiles, 0, dim)
    shape = tiles.shape
    return tiles.reshape(*shape[:dim], shape[dim] * shape[dim + 1], *shape[dim + 2 :])


def gather_directly(array, axis, dim):
    tiles = from_everyone(array, axis)
    return in_order(tiles, dim)


def split_up(array, dim, peers):
    shape = array.shape
    tiles = array.reshape(*shape[:dim], peers, shape[dim] // peers, *shape[dim + 1 :])
    return jnp.moveaxis(tiles, dim, 0)


def sent_and_summed(array, axis, dim):
    tiles = split_up(array, dim, lax.axis_size(axis))
    arrived = lax.all_to_all(tiles, axis, split_axis=0, concat_axis=0, tiled=True)
    return arrived.astype(jnp.float32).sum(axis=0)


def over_axes(array, axes):
    return functools.reduce(lax.psum, axes, array)


def in_one_piece(arrays, axis, dim, along):
    ends, at = ([], 0)
    for a in arrays[:-1]:
        at += a.shape[along]
        ends.append(at)
    both = jnp.concatenate(arrays, axis=along)
    return tuple(jnp.split(lax.all_gather(both, axis, axis=dim, tiled=True), ends, axis=along))


def token_sum(left, right):
    return lax.dot_general(
        left, right, (((0,), (0,)), ((), ())), preferred_element_type=jnp.float32
    )


def moment_update(projected, first, second):
    first_new = 0.8 * first + 0.2 * projected
    second_new = 0.9 * second + 0.1 * projected * projected
    direction = first_new / (jnp.sqrt(second_new) + 1e-08)
    return (first_new, second_new, direction)


def body(
    normed_input,
    query_latent_cotangent,
    key_value_latent_cotangent,
    row_factor,
    query_down_weight,
    key_value_down_weight,
    query_first_moment,
    key_value_first_moment,
    query_second,
    latent_second,
):
    fs_count = lax.axis_size(FS)
    tp_count = lax.axis_size("tp")
    query_width = query_latent_cotangent.shape[1]
    rank_rows = query_first_moment.shape[0]
    factor_whole = gather_directly(row_factor, FS, 0)
    latent_tokens = jnp.dot(normed_input, factor_whole, preferred_element_type=jnp.float32)
    upper_part = latent_tokens.astype(jnp.bfloat16)
    lower_part = (latent_tokens - upper_part.astype(jnp.float32)).astype(jnp.bfloat16)
    both_cotangents = jnp.concatenate([query_latent_cotangent, key_value_latent_cotangent], axis=1)
    projected = sent_and_summed(
        (token_sum(upper_part, both_cotangents) + token_sum(lower_part, both_cotangents)).astype(
            jnp.bfloat16
        ),
        FS,
        0,
    )
    query_first_new, query_second_new, query_dir = moment_update(
        projected[:, :query_width], query_first_moment, query_second
    )
    latent_first_new, latent_second_new, latent_dir = moment_update(
        projected[:, query_width:], key_value_first_moment, latent_second
    )
    query_sq, latent_sq = (
        over_axes(jnp.sum(query_dir * query_dir), FS_TP),
        over_axes(jnp.sum(latent_dir * latent_dir), FS_TP),
    )
    query_count = rank_rows * fs_count * query_width * tp_count
    latent_count = rank_rows * fs_count * key_value_latent_cotangent.shape[1] * tp_count
    query_scale = 0.5 * jnp.sqrt(jnp.float32(query_count)) / jnp.sqrt(query_sq + 1e-06)
    latent_scale = 0.5 * jnp.sqrt(jnp.float32(latent_count)) / jnp.sqrt(latent_sq + 1e-06)
    scaled = jnp.concatenate([query_scale * query_dir, latent_scale * latent_dir], axis=1)
    factor_rows = row_factor.astype(jnp.float32)
    steps = jnp.dot(factor_rows, gather_directly(scaled, FS, 0), preferred_element_type=jnp.float32)
    query_step = steps[:, :query_width]
    latent_step = steps[:, query_width:]
    query_new = query_down_weight - query_step
    latent_new = key_value_down_weight - latent_step
    query_copy, latent_copy = in_one_piece(
        (query_new.astype(jnp.bfloat16), latent_new.astype(jnp.bfloat16)), FS, 0, 1
    )
    return (
        query_new,
        latent_new,
        query_step,
        latent_step,
        query_copy,
        latent_copy,
        query_first_new,
        latent_first_new,
        query_second_new,
        latent_second_new,
    )


def solution(mesh):
    split = Mesh(mesh.devices.reshape(4, 4, 2, mesh.shape["tp"]), ("fs_0", "fs_1", "fs_2", "tp"))
    placed = (
        P(FS, None),
        P(FS, "tp"),
        P(FS, "tp"),
        P(FS, None),
        P(FS, "tp"),
        P(FS, "tp"),
        P(FS, "tp"),
        P(FS, "tp"),
        P(FS, "tp"),
        P(FS, "tp"),
    )
    return jax.shard_map(
        body,
        mesh=split,
        in_specs=placed,
        out_specs=(
            P(FS, "tp"),
            P(FS, "tp"),
            P(FS, "tp"),
            P(FS, "tp"),
            P(None, "tp"),
            P(None, "tp"),
            P(FS, "tp"),
            P(FS, "tp"),
            P(FS, "tp"),
            P(FS, "tp"),
        ),
        check_vma=False,
    )
```

profile of v0, /device:TPU:1, one launch (start us, length us, event | category | flops | bytes accessed | tf_op | source)
XLA Modules:
  0.0 159.6 jit_solution(15034981366741805355)
XLA Ops:
  7.2 0.0 copy-start
  7.2 1.9 %broadcast_in_dim.6 = bf16[32,64,256]{2,1,0:T(8,128)(2,1)} broadcast(bf16[64,256]{1,0:T(8,128)(2,1)} %param.13), dimensions={1,2} | broadcast | bytes 1081344 | tf_op jit(solution)/shard_map/broadcast_in_dim | solution.py:14
  9.1 9.6 %all-to-all-start = ((bf16[32,64,256]{2,1,0:T(8,128)(2,1)}), bf16[32,64,256]{2,1,0:T(8,128)(2,1)S(1)}, u32[]{:S(2)}, u32[]{:S(2)}) async-start(bf16[32,64,256]{2,1,0:T(8,128)(2,1)} %broadcast_in_dim.6), calls=%async_computation | async-start | bytes 2097152 | tf_op jit(solution)/shard_map/all_to_all | solution.py:15
  18.7 0.0 all-gather.2.cloned.1.call-start
  18.8 0.0 copy-done
  18.8 0.6 copy.22
  19.4 16.4 %all-to-all-done = bf16[32,64,256]{2,1,0:T(8,128)(2,1)S(1)} async-done(((bf16[32,64,256]{2,1,0:T(8,128)(2,1)}), bf16[32,64,256]{2,1,0:T(8,128)(2,1)S(1)}, u32[]{:S(2)}, u32[]{:S(2)}) %all-to-all-start) | async-done | bytes 1048608 | tf_op jit(solution)/shard_map/all_to_all | solution.py:15
  35.8 0.0 copy-start.12
  35.8 9.4 %fusion.19 = f32[4608,256]{1,0:T(8,128)S(1)} fusion(bf16[4608,2048]{1,0:T(8,128)(2,1)} %param.10, bf16[2048,256]{1,0:T(8,128)(2,1)S(1)} %bitcast.10), kind=kOutput, calls=%fused_computation.29 | convolution fusion | flops 4831838208 | bytes 24641536 | tf_op jit(solution)/shard_map/dot_general | solution.py:84
  45.2 0.0 copy-done.12
  45.2 1.0 fusion
  46.2 0.0 copy-start.8
  46.2 0.0 copy-start.9
  46.2 0.0 copy-start.10
  46.2 0.0 copy-start.11
  46.2 0.0 copy-start.1
  46.2 0.0 copy-start.2
  46.3 0.0 copy-start.3
  46.3 1.0 fusion.7
  47.2 0.2 copy.23
  47.4 11.8 %all_to_all.15 = bf16[32,8,320]{2,1,0:T(8,128)(2,1)S(1)} all-to-all(bf16[32,8,320]{2,1,0:T(8,128)(2,1)S(1)} %bitcast.11), channel_id=1, replica_groups=mesh['fs_0'=4,'fs_1'=4,'fs_2'=2,'tp'=4] {'fs_0','fs_1','fs_2'}, dimensions={0} | all-to-all | bytes 327680 | tf_op jit(solution)/shard_map/all_to_all | solution.py:37
  59.3 0.0 copy-done.8
  59.3 0.0 copy-done.9
  59.3 0.6 multiply_reduce_fusion
  59.9 0.0 copy-done.10
  59.9 0.0 copy-done.11
  59.9 0.0 copy-start.4
  59.9 0.0 copy-start.5
  59.9 0.7 multiply_reduce_fusion.1
  60.6 0.0 copy-start.6
  60.6 0.0 copy-start.7
  60.6 7.5 %all-reduce.2 = (f32[]{:T(128)}, f32[]{:T(128)}) all-reduce(f32[]{:T(128)} %get-tuple-element.47, f32[]{:T(128)} %get-tuple-element.44), channel_id=1, replica_groups=mesh['fs_0'=4,'fs_1'=4,'fs_2'=2,'tp'=4] {'fs_0'}, use_global_device_ids=true, to_apply=%region_7.0 | all-reduce | flops 2 | bytes 16 | tf_op jit(solution)/shard_map/psum | solution.py:42
  68.1 7.7 %all-reduce.1 = (f32[]{:T(128)}, f32[]{:T(128)}) all-reduce(f32[]{:T(128)} %get-tuple-element.34, f32[]{:T(128)} %get-tuple-element.35), channel_id=1, replica_groups=mesh['fs_0'=4,'fs_1'=4,'fs_2'=2,'tp'=4] {'fs_1'}, use_global_device_ids=true, to_apply=%region_8.0 | all-reduce | flops 2 | bytes 16 | tf_op jit(solution)/shard_map/psum | solution.py:42
  75.8 7.0 %all-reduce.3 = (f32[]{:T(128)}, f32[]{:T(128)}) all-reduce(f32[]{:T(128)} %get-tuple-element.32, f32[]{:T(128)} %get-tuple-element.33), channel_id=1, replica_groups=mesh['fs_0'=4,'fs_1'=4,'fs_2'=2,'tp'=4] {'fs_2'}, use_global_device_ids=true, to_apply=%region_9.0 | all-reduce | flops 2 | bytes 16 | tf_op jit(solution)/shard_map/psum | solution.py:42
  82.8 9.1 %all-reduce = (f32[]{:T(128)}, f32[]{:T(128)}) all-reduce(f32[]{:T(128)} %get-tuple-element.36, f32[]{:T(128)} %get-tuple-element.37), channel_id=1, replica_groups=mesh['fs_0'=4,'fs_1'=4,'fs_2'=2,'tp'=4] {'tp'}, use_global_device_ids=true, to_apply=%region_10.0 | all-reduce | flops 2 | bytes 16 | tf_op jit(solution)/shard_map/psum | solution.py:42
  93.3 0.1 pad_maximum_fusion.8
  93.4 13.3 %all_to_all.16 = bf16[32,8,320]{2,1,0:T(8,128)(2,1)S(1)} all-to-all(bf16[32,8,320]{2,1,0:T(8,128)(2,1)S(1)} %broadcast_in_dim.7), channel_id=1, replica_groups=mesh['fs_0'=4,'fs_1'=4,'fs_2'=2,'tp'=4] {'fs_0','fs_1','fs_2'}, dimensions={0} | all-to-all | bytes 327680 | tf_op jit(solution)/shard_map/all_to_all | solution.py:15
  106.8 0.0 copy-done.1
  106.8 0.2 convolution_bitcast_fusion
  106.9 0.0 copy-done.2
  106.9 0.7 fusion.15
  107.6 0.0 copy-done.3
  107.6 0.7 fusion.16
  108.3 0.7 pad_maximum_fusion.7
  109.0 0.0 all-gather.2.cloned.1.call-update
  109.0 38.9 %all-gather.2.cloned.1.call-done = bf16[2048,320]{1,0:T(8,128)(2,1)} async-done(((bf16[64,320]{1,0:T(8,128)(2,1)}), bf16[2048,320]{1,0:T(8,128)(2,1)}) %all-gather.2.cloned.1.call-update) | async-done | bytes 1310736 | tf_op jit(solution)/shard_map/all_gather | solution.py:51
  148.0 1.3 split.8
  149.2 1.2 copy.24
  150.5 2.2 %split.9 = bf16[2048,128]{1,0:T(8,128)(2,1)} slice(bf16[2048,320]{1,0:T(8,128)(2,1)} %all-gather.2.cloned.1.call-done), slice={[0:2048], [192:320]} | slice | bytes 1048576 | tf_op jit(solution)/shard_map/split | solution.py:51
  152.7 0.0 copy-done.4
  152.7 0.0 copy-done.5
  152.7 0.0 copy-done.6
  152.7 0.0 copy-done.7
  (4 shorter events, 0.1 us)
Async XLA Ops:
  7.2 11.6 %copy-start = (bf16[4608,128]{1,0:T(8,128)(2,1)S(1)}, bf16[4608,128]{1,0:T(8,128)(2,1)}, u32[]{:S(2)}) copy-start(bf16[4608,128]{1,0:T(8,128)(2,1)} %param.12) | copy-start | bytes 3538948
  9.1 26.6 %all-to-all-start = ((bf16[32,64,256]{2,1,0:T(8,128)(2,1)}), bf16[32,64,256]{2,1,0:T(8,128)(2,1)S(1)}, u32[]{:S(2)}, u32[]{:S(2)}) async-start(bf16[32,64,256]{2,1,0:T(8,128)(2,1)} %broadcast_in_dim.6), calls=%async_computation | async-start | bytes 2097152 | tf_op jit(solution)/shard_map/all_to_all | solution.py:15
  18.7 129.2 %all-gather.2.cloned.1.call-start = ((), (), s32[]{:S(2)}) async-start(), calls=%async_computation.3 | async-start | bytes 1622016 | tf_op jit(solution)/shard_map/all_gather | solution.py:51
  35.8 9.4 %copy-start.12 = (bf16[4608,192]{0,1:T(8,128)(2,1)S(1)}, bf16[4608,192]{0,1:T(8,128)(2,1)}, u32[]{:S(2)}) copy-start(bf16[4608,192]{0,1:T(8,128)(2,1)} %param.11) | copy-start | bytes 5308420
  46.2 13.1 %copy-start.8 = (f32[8,192]{1,0:T(8,128)S(1)}, f32[8,192]{1,0:T(8,128)}, u32[]{:S(2)}) copy-start(f32[8,192]{1,0:T(8,128)} %param.18) | copy-start | bytes 18436
  46.2 13.1 %copy-start.9 = (f32[8,192]{1,0:T(8,128)S(1)}, f32[8,192]{1,0:T(8,128)}, u32[]{:S(2)}) copy-start(f32[8,192]{1,0:T(8,128)} %param.16) | copy-start | bytes 18436
  46.2 13.7 %copy-start.10 = (f32[8,128]{1,0:T(8,128)S(1)}, f32[8,128]{1,0:T(8,128)}, u32[]{:S(2)}) copy-start(f32[8,128]{1,0:T(8,128)} %param.19) | copy-start | bytes 12292
  46.2 13.7 %copy-start.11 = (f32[8,128]{1,0:T(8,128)S(1)}, f32[8,128]{1,0:T(8,128)}, u32[]{:S(2)}) copy-start(f32[8,128]{1,0:T(8,128)} %param.17) | copy-start | bytes 12292
  46.2 60.5 %copy-start.1 = (bf16[64,256]{1,0:T(8,128)(2,1)S(1)}, bf16[64,256]{1,0:T(8,128)(2,1)}, u32[]{:S(2)}) copy-start(bf16[64,256]{1,0:T(8,128)(2,1)} %param.13) | copy-start | bytes 98308
  46.2 60.7 %copy-start.2 = (f32[64,192]{1,0:T(8,128)S(1)}, f32[64,192]{1,0:T(8,128)}, u32[]{:S(2)}) copy-start(f32[64,192]{1,0:T(8,128)} %param.14) | copy-start | bytes 147460
  46.3 61.3 %copy-start.3 = (f32[64,128]{1,0:T(8,128)S(1)}, f32[64,128]{1,0:T(8,128)}, u32[]{:S(2)}) copy-start(f32[64,128]{1,0:T(8,128)} %param.15) | copy-start | bytes 98308
  59.9 92.8 %copy-start.4 = (f32[8,192]{1,0:T(8,128)}, f32[8,192]{1,0:T(8,128)S(1)}, u32[]{:S(2)}) copy-start(f32[8,192]{1,0:T(8,128)S(1)} %get-tuple-element.45) | copy-start | bytes 18436
  59.9 92.8 %copy-start.5 = (f32[8,192]{1,0:T(8,128)}, f32[8,192]{1,0:T(8,128)S(1)}, u32[]{:S(2)}) copy-start(f32[8,192]{1,0:T(8,128)S(1)} %get-tuple-element.46) | copy-start | bytes 18436
  60.6 92.1 %copy-start.6 = (f32[8,128]{1,0:T(8,128)}, f32[8,128]{1,0:T(8,128)S(1)}, u32[]{:S(2)}) copy-start(f32[8,128]{1,0:T(8,128)S(1)} %get-tuple-element.48) | copy-start | bytes 12292
  60.6 92.1 %copy-start.7 = (f32[8,128]{1,0:T(8,128)}, f32[8,128]{1,0:T(8,128)S(1)}, u32[]{:S(2)}) copy-start(f32[8,128]{1,0:T(8,128)S(1)} %get-tuple-element.49) | copy-start | bytes 12292
Sparse Core Ops, SparseCore 0:
  109.1 38.7 all-gather.1
where the time goes:
time: 160 us
  blocking collectives  56.4 us (35%)
  waiting for transfers between devices  55.3 us (35%)
  between operations  15.6 us (10%)
  matrix products  11.5 us (7%)
  starting transfers between devices  9.63 us (6%)
  local copies, waits for them, and re-layouts  7.56 us (5%)
  other arithmetic  3.52 us (2%)
    all_gather x1, waiting for transfers between devices, in_one_piece(): lax.all_gather(both, axis, axis=dim, tiled=True)  38.9 us
    psum x4, blocking collectives, over_axes(): return functools.reduce(lax.psum, axes, array)  31.2 us
    all_to_all x1, waiting for transfers between devices, from_everyone(): return lax.all_to_all(copies, axis, split_axis=0, concat_axis=0, tiled=True)  16.4 us
    all_to_all x1, blocking collectives, from_everyone(): return lax.all_to_all(copies, axis, split_axis=0, concat_axis=0, tiled=True)  13.3 us
    all_to_all x1, blocking collectives, sent_and_summed(): lax.all_to_all(tiles, axis, split_axis=0, concat_axis=0, tiled=True)  11.8 us
    all_to_all x1, starting transfers between devices, from_everyone(): return lax.all_to_all(copies, axis, split_axis=0, concat_axis=0, tiled=True)  9.59 us
    dot_general x1, matrix products, body(): jnp.dot(normed_input, factor_whole, preferred_element_type=jnp.float32)  9.4 us
    split x2, local copies, waits for them, and re-layouts, in_one_piece(): jnp.split(lax.all_gather(both, axis, axis=dim, tiled=True), ends, axis=al...  3.52 us
  transfers between devices with their start and end apart: 2, of which 2 were waited for; matrix products, arithmetic and copies ran while one was open for 0% of the time, Pallas kernels for 0%

commit v1 on v0

v1 whole, which is shorter than its diff:
```python
import functools

import jax
import jax.numpy as jnp
from jax import lax
from jax.experimental import pallas as pl
from jax.experimental.pallas import tpu as pltpu
from jax.sharding import PartitionSpec as P

MESH = pl.DeviceIdType.MESH
Z, Y, CORES, TP = 4, 4, 2, 4
FS = Z * Y * CORES
BF16, F32 = jnp.bfloat16, jnp.float32


def remote(src, dst, send, recv, **where):
    return pltpu.make_async_remote_copy(
        src_ref=src, dst_ref=dst, send_sem=send, recv_sem=recv, device_id=where, device_id_type=MESH
    )


def exchange_kernel(
    chunk,
    x_hbm, cq_hbm, ck_hbm, f_hbm, wq_hbm, wk_hbm, mq_hbm, mk_hbm, vq_hbm, vk_hbm,
    f_all, w_all, d_all, squares, total,
    x, cq, ck, ct, grad, gradh, wq, wk, mq, mk, vq, vk, part, parts,
    x_sem, small_sem, f_sem, gather_send, gather_recv, sum_sem, dir_sem, tp_sem,
):
    steps = x.shape[0] // chunk
    kv, qw = ck.shape[1], cq.shape[1]
    width = kv + qw
    me = lax.axis_index("fs")
    tp = lax.axis_index("tp")
    z, y, c = me // (Y * CORES), (me // CORES) % Y, me % CORES

    barrier = pltpu.get_barrier_semaphore()

    @pl.loop(1, FS)
    def _(d):
        pl.semaphore_signal(barrier, 1, device_id={"fs": (me + d) % FS}, device_id_type=MESH)

    @pl.loop(1, TP)
    def _(d):
        pl.semaphore_signal(barrier, 1, device_id={"tp": (tp + d) % TP}, device_id_type=MESH)

    own_f = pltpu.make_async_copy(f_hbm, f_all.at[z, y, c], f_sem)
    own_f.start()
    small = [
        pltpu.make_async_copy(a, b, small_sem.at[i])
        for i, (a, b) in enumerate(
            ((wq_hbm, wq), (wk_hbm, wk), (mq_hbm, mq), (mk_hbm, mk), (vq_hbm, vq), (vk_hbm, vk))
        )
    ]
    for copy in small[:2]:
        copy.start()

    def chunk_copies(k):
        rows = pl.ds(pl.multiple_of(k * chunk, chunk), chunk)
        return [
            pltpu.make_async_copy(a.at[rows], b.at[rows], x_sem.at[k, i])
            for i, (a, b) in enumerate(((cq_hbm, cq), (ck_hbm, ck), (x_hbm, x)))
        ]

    @pl.loop(0, steps)
    def _(k):
        for copy in chunk_copies(k):
            copy.start()

    for copy in small[2:]:
        copy.start()
    grad[...] = jnp.zeros_like(grad)
    own_f.wait()
    small[0].wait()
    small[1].wait()
    w_all[z, y, c, :, :kv] = wk[...].astype(BF16)
    w_all[z, y, c, :, kv:width] = wq[...].astype(BF16)
    pl.semaphore_wait(barrier, FS + TP - 2)

    half = f_all.shape[3] // 2
    lower, upper = pl.ds(0, half), pl.ds(half, half)
    stage_sem = lambda stage, which, lane: (
        gather_send.at[stage, which, lane],
        gather_recv.at[stage, which, lane],
    )
    peer_y = lambda d: (z * Y + (y + d) % Y) * CORES + c
    peer_z = lambda d: ((z + d) % Z * Y + y) * CORES + c

    def first_stage(a, which):
        for d in range(1, Y):
            block = a.at[z, y, c, lower]
            remote(block, block, *stage_sem(0, which, 0), fs=peer_y(d)).start()
        for d in range(1, Z):
            block = a.at[z, y, c, upper]
            remote(block, block, *stage_sem(0, which, 1), fs=peer_z(d)).start()

    def first_wait(a, which):
        seen = a.at[0, pl.ds(0, Y - 1), c, lower]
        remote(seen, seen, *stage_sem(0, which, 0), fs=peer_y(1)).wait()
        seen = a.at[pl.ds(0, Z - 1), 0, c, upper]
        remote(seen, seen, *stage_sem(0, which, 1), fs=peer_z(1)).wait()

    def second_stage(a, which):
        for d in range(1, Z):
            block = a.at[z, :, c, lower]
            remote(block, block, *stage_sem(1, which, 0), fs=peer_z(d)).start()
        for d in range(1, Y):
            block = a.at[:, y, c, upper]
            remote(block, block, *stage_sem(1, which, 1), fs=peer_y(d)).start()

    def second_wait(a, which):
        seen = a.at[pl.ds(0, Z - 1), :, c, lower]
        remote(seen, seen, *stage_sem(1, which, 0), fs=peer_z(1)).wait()
        seen = a.at[:, pl.ds(0, Y - 1), c, upper]
        remote(seen, seen, *stage_sem(1, which, 1), fs=peer_y(1)).wait()

    def partner_stage(a, which):
        block = a.at[:, :, c]
        remote(block, block, *stage_sem(2, which, 0), fs=me + 1 - 2 * c).start()

    def partner_wait(a, which):
        block = a.at[:, :, c]
        remote(block, block, *stage_sem(2, which, 0), fs=me + 1 - 2 * c).wait()

    first_stage(f_all, 0)
    first_stage(w_all, 1)

    @pl.loop(0, steps)
    def _(k):
        for copy in chunk_copies(k):
            copy.wait()
        rows = pl.ds(pl.multiple_of(k * chunk, chunk), chunk)
        ct[:kv, :] = ck[rows, :].T
        ct[kv:width, :] = cq[rows, :].T
        grad[...] += jnp.dot(ct[...], x[rows, :], preferred_element_type=F32)

        @pl.when(k == 3)
        def _():
            first_wait(f_all, 0)
            second_stage(f_all, 0)
            first_wait(w_all, 1)
            second_stage(w_all, 1)

    gradh[...] = grad[...].astype(BF16)
    second_wait(f_all, 0)
    partner_stage(f_all, 0)
    second_wait(w_all, 1)
    partner_stage(w_all, 1)
    partner_wait(f_all, 0)
    projected = jnp.dot(
        gradh[...], f_all[...].reshape(gradh.shape[1], f_all.shape[-1]), preferred_element_type=F32
    )
    rank = projected.shape[1] // FS
    part[:, :, :width] = projected.T.reshape(FS, rank, width).astype(BF16)

    @pl.loop(1, FS)
    def _(d):
        to = (me + d) % FS
        remote(part.at[to], parts.at[d - 1], sum_sem.at[0], sum_sem.at[1], fs=to).start()

    for copy in small[2:]:
        copy.wait()
    seen = parts
    remote(seen, seen, sum_sem.at[0], sum_sem.at[1], fs=me + 1 - 2 * c).wait()
    summed = part[me].astype(F32) + parts[...].astype(F32).sum(axis=0)
    total[...] = summed
    for low, high, first, second in ((0, kv, mk, vk), (kv, width, mq, vq)):
        got = summed[:, low:high]
        first_new = 0.8 * first[...] + 0.2 * got
        second_new = 0.9 * second[...] + 0.1 * got * got
        d_all[me, :, low:high] = (first_new / (jnp.sqrt(second_new) + 1e-08)).astype(BF16)

    @pl.loop(1, FS)
    def _(d):
        mine = d_all.at[me]
        remote(mine, mine, dir_sem.at[0], dir_sem.at[1], fs=(me + d) % FS).start()

    partner_wait(w_all, 1)
    seen = d_all.at[pl.ds(0, FS - 1)]
    remote(seen, seen, dir_sem.at[0], dir_sem.at[1], fs=me + 1 - 2 * c).wait()
    every = d_all[...].astype(F32)
    every = every * every
    sum_kv = jnp.sum(every[:, :, :kv], axis=(0, 1, 2), keepdims=True)[0]
    sum_q = jnp.sum(every[:, :, kv:width], axis=(0, 1, 2), keepdims=True)[0]
    which = lax.broadcasted_iota(jnp.int32, squares.shape[1:], 0)
    squares[tp] = jnp.where(which == 0, sum_kv, sum_q)

    @pl.loop(1, TP)
    def _(d):
        mine = squares.at[tp]
        remote(mine, mine, tp_sem.at[0], tp_sem.at[1], tp=(tp + d) % TP).start()

    seen = squares.at[pl.ds(0, TP - 1)]
    remote(seen, seen, tp_sem.at[0], tp_sem.at[1], tp=(tp + 1) % TP).wait()


def update_kernel(
    counts,
    f_all, w_all, d_all, squares, total, f_own, wq, wk, mq, mk, vq, vk,
    q_new, l_new, q_step, l_step, q_copy, l_copy, q_first, l_first, q_second, l_second,
):
    kv = wk.shape[1]
    width = kv + wq.shape[1]
    sums = squares[0] + squares[1] + squares[2] + squares[3]
    scales = [
        0.5 * jnp.sqrt(jnp.full((1, 1), counts[i], F32)) / jnp.sqrt(sums[i : i + 1, :1] + 1e-06)
        for i in range(2)
    ]
    summed = total[...]
    for low, high, first, second, first_new, second_new in (
        (0, kv, mk, vk, l_first, l_second),
        (kv, width, mq, vq, q_first, q_second),
    ):
        got = summed[:, low:high]
        first_new[...] = 0.8 * first[...] + 0.2 * got
        second_new[...] = 0.9 * second[...] + 0.1 * got * got
    rank = f_all.shape[-1]
    rows = 1
    for n in f_all.shape[:-1]:
        rows *= n
    directions = d_all[...].astype(F32).reshape(rank, d_all.shape[-1])[:, :width].astype(BF16)
    own = jnp.dot(f_own[...], directions, preferred_element_type=F32)
    for low, high, scale, weight, new, step in (
        (0, kv, scales[0], wk, l_new, l_step),
        (kv, width, scales[1], wq, q_new, q_step),
    ):
        taken = own[:, low:high] * scale
        step[...] = taken
        new[...] = weight[...] - taken
    whole = jnp.dot(f_all[...].reshape(rows, rank), directions, preferred_element_type=F32)
    weights = w_all[...].reshape(rows, w_all.shape[-1])
    l_copy[...] = (weights[:, :kv].astype(F32) - whole[:, :kv] * scales[0]).astype(BF16)
    q_copy[...] = (weights[:, kv:width].astype(F32) - whole[:, kv:] * scales[1]).astype(BF16)


def body(x, cq, ck, f, wq, wk, mq, mk, vq, vk):
    tokens, model = x.shape
    rows, rank = f.shape
    qw, kv = cq.shape[1], ck.shape[1]
    width = kv + qw
    lanes = -(-width // 128) * 128
    mine = rank // FS
    chunk = 512
    steps = tokens // chunk
    anywhere = pl.BlockSpec(memory_space=pl.ANY)
    vmem = pl.BlockSpec(memory_space=pltpu.VMEM)
    shape = jax.ShapeDtypeStruct
    dma = pltpu.SemaphoreType.DMA
    gathered = pl.pallas_call(
        functools.partial(exchange_kernel, chunk),
        out_shape=(
            shape((Z, Y, CORES, rows, rank), BF16),
            shape((Z, Y, CORES, rows, lanes), BF16),
            shape((FS, mine, lanes), BF16),
            shape((TP, 8, 128), F32),
            shape((mine, lanes), F32),
        ),
        in_specs=[anywhere] * 10,
        out_specs=(vmem,) * 5,
        scratch_shapes=[
            pltpu.VMEM((tokens, model), BF16),
            pltpu.VMEM((tokens, qw), BF16),
            pltpu.VMEM((tokens, kv), BF16),
            pltpu.VMEM((width, chunk), BF16),
            pltpu.VMEM((width, model), F32),
            pltpu.VMEM((width, model), BF16),
            pltpu.VMEM((rows, qw), F32),
            pltpu.VMEM((rows, kv), F32),
            pltpu.VMEM((mine, qw), F32),
            pltpu.VMEM((mine, kv), F32),
            pltpu.VMEM((mine, qw), F32),
            pltpu.VMEM((mine, kv), F32),
            pltpu.VMEM((FS, mine, lanes), BF16),
            pltpu.VMEM((FS - 1, mine, lanes), BF16),
            dma((steps, 3)),
            dma((6,)),
            dma,
            dma((3, 2, 2)),
            dma((3, 2, 2)),
            dma((2,)),
            dma((2,)),
            dma((2,)),
        ],
        compiler_params=pltpu.CompilerParams(
            collective_id=0, has_side_effects=True, vmem_limit_bytes=44 * 1024 * 1024
        ),
        name="exchange",
    )(x, cq, ck, f, wq, wk, mq, mk, vq, vk)
    counts = (rank * kv * TP, rank * qw * TP)
    model_rows = rows * FS
    lik = lambda a: shape(a.shape, a.dtype)
    return pl.pallas_call(
        functools.partial(update_kernel, counts),
        out_shape=(
            lik(wq), lik(wk), lik(wq), lik(wk),
            shape((model_rows, qw), BF16), shape((model_rows, kv), BF16),
            lik(mq), lik(mk), lik(vq), lik(vk),
        ),
        in_specs=[vmem] * 12,
        out_specs=(vmem,) * 10,
        name="update",
    )(*gathered[:4], gathered[4][:, :width], f, wq, wk, mq, mk, vq, vk)


def solution(mesh):
    return jax.shard_map(
        body,
        mesh=mesh,
        in_specs=(P("fs", None), P("fs", "tp"), P("fs", "tp"), P("fs", None)) + (P("fs", "tp"),) * 6,
        out_specs=(P("fs", "tp"),) * 4 + (P(None, "tp"),) * 2 + (P("fs", "tp"),) * 4,
        check_vma=False,
    )
```

time: 160 us -> 54.4 us (0.34)
  blocking collectives: 56.4 us -> 0 us
  waiting for transfers between devices: 55.3 us -> 0 us
  Pallas kernels: 0 us -> 40.5 us
  between operations: 15.6 us -> 0.73 us
  matrix products: 11.5 us -> 0 us
  starting transfers between devices: 9.63 us -> 0 us
  local copies, waits for them, and re-layouts: 7.56 us -> 12.7 us
  other arithmetic: 3.52 us -> 0 us
    pallas_call x0 -> x2, Pallas kernels: none -> 40.5 us  [the longest x1 36.8 us: body(): pl.pallas_call(functools.partial(exchange_kernel, chunk), out_shape=(shap...]
    all_gather x1 -> x0, waiting for transfers between devices: 38.9 us -> none  [in_one_piece(): lax.all_gather(both, axis, axis=dim, tiled=True)]
    psum x4 -> x0, blocking collectives: 31.2 us -> none  [over_axes(): return functools.reduce(lax.psum, axes, array)]
    all_to_all x2 -> x0, blocking collectives: 25.2 us -> none  [the longest x1 13.3 us: from_everyone(): return lax.all_to_all(copies, axis, split_axis=0, concat_axis=0, tiled=True)]
    all_to_all x1 -> x0, waiting for transfers between devices: 16.4 us -> none  [from_everyone(): return lax.all_to_all(copies, axis, split_axis=0, concat_axis=0, tiled=True)]
    dot_general x4 -> x0, matrix products: 11.5 us -> none  [the longest x1 9.4 us: body(): jnp.dot(normed_input, factor_whole, preferred_element_type=jnp.float32)]
    all_to_all x1 -> x0, starting transfers between devices: 9.59 us -> none  [from_everyone(): return lax.all_to_all(copies, axis, split_axis=0, concat_axis=0, tiled=True)]
    unnamed x28 -> x27, local copies, waits for them, and re-layouts: 1.91 us -> 10.5 us
  transfers between devices with their start and end apart: 2 -> 0, of which waited for: 2 -> 0; matrix products, arithmetic and copies ran while one was open for 0% -> 0% of each run, Pallas kernels for 0% -> 0%
where the time goes in v1:
time: 54.4 us; the launch traced here: 53.9 us
  Pallas kernels  40.5 us (74%)
  local copies, waits for them, and re-layouts  12.7 us (23%)
  between operations  0.73 us (1%)
    pallas_call x1, Pallas kernels, body(): pl.pallas_call(functools.partial(exchange_kernel, chunk), out_shape=(shap...  36.8 us
    unnamed x27, local copies, waits for them, and re-layouts  10.5 us
    pallas_call x1, Pallas kernels, body(): pl.pallas_call(functools.partial(update_kernel, counts), out_shape=(lik(w...  3.69 us
    pallas_call x1, local copies, waits for them, and re-layouts, body(): pl.pallas_call(functools.partial(update_kernel, counts), out_shape=(lik(w...  2.19 us

profile of v1, /device:TPU:1, one launch (start us, length us, event | category | flops | bytes accessed | tf_op | source)
XLA Modules:
  0.0 53.9 jit_solution(1782198259382020690)
XLA Ops:
  0.6 0.0 copy-start.8
  0.7 0.0 copy-start.7
  0.7 0.0 copy-start.1
  0.7 2.8 %copy.20.cq_hbm = bf16[4608,192]{1,0:T(8,128)(2,1)S(1)} copy(bf16[4608,192]{0,1:T(8,128)(2,1)} %param.11) | data formatting | bytes 3538944 | tf_op args[1]
  3.5 0.0 copy-done.8
  3.5 0.0 copy-done.7
  3.5 0.0 copy-done.1
  3.5 0.0 copy-start.3
  3.5 0.8 %copy-done.3 = f32[64,192]{1,0:T(8,128)S(1)} copy-done((f32[64,192]{1,0:T(8,128)S(1)}, f32[64,192]{1,0:T(8,128)}, u32[]{:S(2)}) %copy-start.3) | copy-done | bytes 49176
  4.3 0.0 copy-start.5
  4.4 0.8 %copy-done.5 = bf16[64,256]{1,0:T(8,128)(2,1)S(1)} copy-done((bf16[64,256]{1,0:T(8,128)(2,1)S(1)}, bf16[64,256]{1,0:T(8,128)(2,1)}, u32[]{:S(2)}) %copy-start.5) | copy-done | bytes 32792
  5.1 0.0 copy-start.6
  5.1 0.8 %copy-done.6 = f32[64,128]{1,0:T(8,128)S(1)} copy-done((f32[64,128]{1,0:T(8,128)S(1)}, f32[64,128]{1,0:T(8,128)}, u32[]{:S(2)}) %copy-start.6) | copy-done | bytes 32792
  5.9 0.0 copy-start.10
  5.9 0.7 %copy-done.10 = f32[8,128]{1,0:T(8,128)S(1)} copy-done((f32[8,128]{1,0:T(8,128)S(1)}, f32[8,128]{1,0:T(8,128)}, u32[]{:S(2)}) %copy-start.10) | copy-done | bytes 4120
  6.6 0.0 copy-start.11
  6.6 0.7 %copy-done.11 = f32[8,128]{1,0:T(8,128)S(1)} copy-done((f32[8,128]{1,0:T(8,128)S(1)}, f32[8,128]{1,0:T(8,128)}, u32[]{:S(2)}) %copy-start.11) | copy-done | bytes 4120
  7.2 36.8 %exchange.1 = (bf16[4,4,2,64,256]{4,3,2,1,0:T(8,128)(2,1)S(1)}, bf16[4,4,2,64,384]{4,3,2,1,0:T(8,128)(2,1)S(1)}, bf16[32,8,384]{2,1,0:T(8,128)(2,1)S(1)}, f32[4,8,128]{2,1,0:T(8,128)S(1)}, f32[8,384]{1,0:T(8,128)S(1)}) custom-call(bf16[4608,2048]{1,0:T(8,128)(2,1)} %x_hbm.1, bf16[4608,192]{1,0:T(8,128)(2,1)S(1)} %copy.20.cq_hbm, ...), custom_call_target="tpu_custom_call" | custom-call | tf_op jit(solution)/shard_map/exchange/pallas_call | solution.py:248
  44.0 0.0 copy-start
  44.0 1.2 %copy-done = bf16[4,4,2,64,384]{4,3,2,1,0:T(8,128)(2,1)} copy-done((bf16[4,4,2,64,384]{4,3,2,1,0:T(8,128)(2,1)}, bf16[4,4,2,64,384]{4,3,2,1,0:T(8,128)(2,1)S(1)}, u32[]{:S(2)}) %copy-start) | copy-done | bytes 1572888
  45.2 0.0 copy-start.2
  45.2 1.0 %copy-done.2 = bf16[4,4,2,64,256]{4,3,2,1,0:T(8,128)(2,1)} copy-done((bf16[4,4,2,64,256]{4,3,2,1,0:T(8,128)(2,1)}, bf16[4,4,2,64,256]{4,3,2,1,0:T(8,128)(2,1)S(1)}, u32[]{:S(2)}) %copy-start.2) | copy-done | bytes 1048600
  46.2 0.0 copy-start.4
  46.2 0.7 %copy-done.4 = bf16[32,8,384]{2,1,0:T(8,128)(2,1)} copy-done((bf16[32,8,384]{2,1,0:T(8,128)(2,1)}, bf16[32,8,384]{2,1,0:T(8,128)(2,1)S(1)}, u32[]{:S(2)}) %copy-start.4) | copy-done | bytes 196632
  46.9 0.0 copy-start.9
  46.9 0.6 %copy-done.9 = f32[4,8,128]{2,1,0:T(8,128)} copy-done((f32[4,8,128]{2,1,0:T(8,128)}, f32[4,8,128]{2,1,0:T(8,128)S(1)}, u32[]{:S(2)}) %copy-start.9) | copy-done | bytes 16408
  47.5 0.0 copy-start.12
  47.5 0.6 %copy-done.12 = f32[8,384]{1,0:T(8,128)} copy-done((f32[8,384]{1,0:T(8,128)}, f32[8,384]{1,0:T(8,128)S(1)}, u32[]{:S(2)}) %copy-start.12) | copy-done | bytes 12312
  48.1 3.7 %update.1 = (f32[64,192]{1,0:T(8,128)}, f32[64,128]{1,0:T(8,128)}, f32[64,192]{1,0:T(8,128)}, f32[64,128]{1,0:T(8,128)}, bf16[2048,192]{1,0:T(8,128)(2,1)}, /*in...) custom-call(bf16[4,4,2,64,256]{4,3,2,1,0:T(8,128)(2,1)} %copy-done.2, ...), custom_call_target="tpu_custom_call" | custom-call | tf_op jit(solution)/shard_map/update/pallas_call | solution.py:291
  51.8 2.2 %copy.21 = bf16[2048,192]{0,1:T(8,128)(2,1)} copy(bf16[2048,192]{1,0:T(8,128)(2,1)} %get-tuple-element.24) | data formatting | bytes 1572864 | tf_op jit(solution)/shard_map/update/pallas_call | solution.py:291
Async XLA Ops:
  0.6 2.8 %copy-start.8 = (f32[8,192]{1,0:T(8,128)S(1)}, f32[8,192]{1,0:T(8,128)}, u32[]{:S(2)}) copy-start(f32[8,192]{1,0:T(8,128)} %vq.1) | copy-start | bytes 18436
  0.7 2.8 %copy-start.7 = (f32[8,192]{1,0:T(8,128)S(1)}, f32[8,192]{1,0:T(8,128)}, u32[]{:S(2)}) copy-start(f32[8,192]{1,0:T(8,128)} %mq.1) | copy-start | bytes 18436
  0.7 2.8 %copy-start.1 = (bf16[4608,128]{1,0:T(8,128)(2,1)S(1)}, bf16[4608,128]{1,0:T(8,128)(2,1)}, u32[]{:S(2)}) copy-start(bf16[4608,128]{1,0:T(8,128)(2,1)} %ck_hbm.1) | copy-start | bytes 3538948
  3.5 0.8 %copy-start.3 = (f32[64,192]{1,0:T(8,128)S(1)}, f32[64,192]{1,0:T(8,128)}, u32[]{:S(2)}) copy-start(f32[64,192]{1,0:T(8,128)} %wq.1) | copy-start | bytes 147460
  4.3 0.8 %copy-start.5 = (bf16[64,256]{1,0:T(8,128)(2,1)S(1)}, bf16[64,256]{1,0:T(8,128)(2,1)}, u32[]{:S(2)}) copy-start(bf16[64,256]{1,0:T(8,128)(2,1)} %f_own.1) | copy-start | bytes 98308
  5.1 0.8 %copy-start.6 = (f32[64,128]{1,0:T(8,128)S(1)}, f32[64,128]{1,0:T(8,128)}, u32[]{:S(2)}) copy-start(f32[64,128]{1,0:T(8,128)} %wk.1) | copy-start | bytes 98308
  5.9 0.7 %copy-start.10 = (f32[8,128]{1,0:T(8,128)S(1)}, f32[8,128]{1,0:T(8,128)}, u32[]{:S(2)}) copy-start(f32[8,128]{1,0:T(8,128)} %mk.1) | copy-start | bytes 12292
  6.6 0.7 %copy-start.11 = (f32[8,128]{1,0:T(8,128)S(1)}, f32[8,128]{1,0:T(8,128)}, u32[]{:S(2)}) copy-start(f32[8,128]{1,0:T(8,128)} %vk.1) | copy-start | bytes 12292
  44.0 1.2 %copy-start = (bf16[4,4,2,64,384]{4,3,2,1,0:T(8,128)(2,1)}, bf16[4,4,2,64,384]{4,3,2,1,0:T(8,128)(2,1)S(1)}, u32[]{:S(2)}) copy-start(bf16[4,4,2,64,384]{4,3,2,1,0:T(8,128)(2,1)S(1)} %get-tuple-element.16.w_all) | copy-start | bytes 4718596
  45.2 1.0 %copy-start.2 = (bf16[4,4,2,64,256]{4,3,2,1,0:T(8,128)(2,1)}, bf16[4,4,2,64,256]{4,3,2,1,0:T(8,128)(2,1)S(1)}, u32[]{:S(2)}) copy-start(bf16[4,4,2,64,256]{4,3,2,1,0:T(8,128)(2,1)S(1)} %get-tuple-element.15.f_all) | copy-start | bytes 3145732
  46.2 0.7 %copy-start.4 = (bf16[32,8,384]{2,1,0:T(8,128)(2,1)}, bf16[32,8,384]{2,1,0:T(8,128)(2,1)S(1)}, u32[]{:S(2)}) copy-start(bf16[32,8,384]{2,1,0:T(8,128)(2,1)S(1)} %get-tuple-element.17.d_all) | copy-start | bytes 589828
  46.9 0.6 %copy-start.9 = (f32[4,8,128]{2,1,0:T(8,128)}, f32[4,8,128]{2,1,0:T(8,128)S(1)}, u32[]{:S(2)}) copy-start(f32[4,8,128]{2,1,0:T(8,128)S(1)} %get-tuple-element.18.squares) | copy-start | bytes 49156
  47.5 0.6 %copy-start.12 = (f32[8,384]{1,0:T(8,128)}, f32[8,384]{1,0:T(8,128)S(1)}, u32[]{:S(2)}) copy-start(f32[8,384]{1,0:T(8,128)S(1)} %get-tuple-element.19) | copy-start | bytes 36868

commit v2 on v1

v2 whole, which is shorter than its diff:
```python
import functools

import jax
import jax.numpy as jnp
from jax import lax
from jax.experimental import pallas as pl
from jax.experimental.pallas import tpu as pltpu
from jax.sharding import PartitionSpec as P

MESH = pl.DeviceIdType.MESH
Z, Y, CORES, TP = 4, 4, 2, 4
FS = Z * Y * CORES
BF16, F32 = jnp.bfloat16, jnp.float32
CHUNK = 768
NEAR_AT, FAR_AT, W_NEAR_AT, W_FAR_AT, PAIR_AT = 3, 3, 4, 5, 5
SELF = 20
NEAREST = sorted(range(FS), key=lambda i: min(i // 8, 4 - i // 8) + min(i // 2 % 4, 4 - i // 2 % 4))


def remote(src, dst, send, recv, **where):
    return pltpu.make_async_remote_copy(
        src_ref=src, dst_ref=dst, send_sem=send, recv_sem=recv, device_id=where, device_id_type=MESH
    )


def exchange_kernel(
    x_hbm, cq_hbm, ck_hbm, f_hbm, wq_hbm, wk_hbm, mq_hbm, mk_hbm, vq_hbm, vk_hbm,
    w_all, q_weights, l_steps, q_steps, own_steps, squares, total,
    f_all, d_all, x, ck, ct, grad, gradh, wq, wk, mq, mk, vq, vk, part, parts,
    x_sem, small_sem, f_sem, own_send, own_recv, relay_send, relay_recv, pair_sem, sum_sem, dir_sem, square_sem,
):
    kv, qw = ck.shape[1], cq_hbm.shape[0]
    width = kv + qw
    me = lax.axis_index("fs")
    tp = lax.axis_index("tp")
    z, y, c = me // (Y * CORES), (me // CORES) % Y, me % CORES
    at = lambda dz, dy, dc: (((z + dz) % Z) * Y + (y + dy) % Y) * CORES + (c + dc) % CORES
    partner = at(0, 0, 1)

    def plane(i):
        return at((2 + i // (Y * CORES)) % Z, (2 + i // CORES) % Y, i % CORES)

    def to_plane(send):
        @pl.loop(0, FS)
        def _(i):
            pl.when(i != SELF)(functools.partial(send, i))

    barrier = pltpu.get_barrier_semaphore()
    axis_peers = [at(0, d, 0) for d in range(1, Y)] + [at(d, 0, 0) for d in range(1, Z)] + [partner]
    for peer in axis_peers:
        pl.semaphore_signal(barrier, 1, device_id={"fs": peer}, device_id_type=MESH)
    for d in range(1, TP):
        pl.semaphore_signal(barrier, 1, device_id={"tp": (tp + d) % TP}, device_id_type=MESH)

    own_f = pltpu.make_async_copy(f_hbm, f_all.at[z, y, c], f_sem)
    own_f.start()
    small = [
        pltpu.make_async_copy(a, b, small_sem.at[i])
        for i, (a, b) in enumerate(
            ((wq_hbm, wq), (wk_hbm, wk), (mq_hbm, mq), (mk_hbm, mk), (vq_hbm, vq), (vk_hbm, vk))
        )
    ]
    for copy in small[:2]:
        copy.start()

    steps = x.shape[0] // CHUNK
    span = lambda k: pl.ds(pl.multiple_of(k * CHUNK, CHUNK), CHUNK)
    cq_copy = lambda k: pltpu.make_async_copy(
        cq_hbm.at[:, span(k)], ct.at[pl.ds(kv, qw), span(k)], x_sem.at[k, 0]
    )
    ck_copy = lambda k: pltpu.make_async_copy(ck_hbm.at[span(k)], ck.at[span(k)], x_sem.at[k, 1])
    x_copy = lambda k: pltpu.make_async_copy(x_hbm.at[span(k)], x.at[span(k)], x_sem.at[k, 2])

    @pl.loop(0, steps)
    def _(k):
        ck_copy(k).start()
        cq_copy(k).start()
        x_copy(k).start()

    for copy in small[2:]:
        copy.start()

    lower, upper = pl.ds(0, f_all.shape[3] // 2), pl.ds(f_all.shape[3] // 2, f_all.shape[3] // 2)

    def own_copy(a, which, along, d, slot):
        where = at(0, d, 0) if along else at(d, 0, 0)
        block = a.at[slot]
        return remote(
            block, block, own_send.at[which, along, d - 1], own_recv.at[which, along, d - 1], fs=where
        )

    def own_start(a, which):
        for d in (2, 1, 3):
            for along in range(2):
                own_copy(a, which, along, d, (z, y, c)).start()

    def relay_copy(a, which, along, d, e, slot):
        where = at(0, e, 0) if along else at(e, 0, 0)
        block = a.at[slot + ((upper if along else lower),)]
        return remote(
            block, block, relay_send.at[which, along], relay_recv.at[which, along], fs=where
        )

    def relay(a, which, distances):
        for d in distances:
            came_y = (z, (y - d + Y) % Y, c)
            came_z = ((z - d + Z) % Z, y, c)
            own_copy(a, which, 1, d, came_y).wait_recv()
            own_copy(a, which, 0, d, came_z).wait_recv()
            for e in (2, 1, 3):
                relay_copy(a, which, 0, d, e, came_y).start()
                relay_copy(a, which, 1, d, e, came_z).start()

    def relay_wait(a, which):
        for along in range(2):
            seen = a.at[pl.ds(0, 3), pl.ds(0, 3), c, lower]
            remote(seen, seen, relay_send.at[which, along], relay_recv.at[which, along], fs=partner).wait()
        for d in (1, 2, 3):
            for along in range(2):
                own_copy(a, which, along, d, (z, y, c)).wait_send()

    def pair_copy(a, which):
        block = a.at[:, :, c]
        return remote(block, block, pair_sem.at[which, 0], pair_sem.at[which, 1], fs=partner)

    def pair_start(a, which):
        relay_wait(a, which)
        pair_copy(a, which).start()

    own_f.wait()
    pl.semaphore_wait(barrier, len(axis_peers) + TP - 1)
    own_start(f_all, 0)
    small[0].wait()
    small[1].wait()
    w_all[z, y, c, :, :kv] = wk[...].astype(BF16)
    w_all[z, y, c, :, kv:width] = wq[...].astype(BF16)
    grad[...] = jnp.zeros_like(grad)
    own_start(w_all, 1)

    @pl.loop(0, steps)
    def _(k):
        for step, a, which, distances in (
            (NEAR_AT, f_all, 0, (1, 3)),
            (FAR_AT, f_all, 0, (2,)),
            (W_NEAR_AT, w_all, 1, (1, 3)),
            (W_FAR_AT, w_all, 1, (2,)),
        ):
            pl.when(k == step)(functools.partial(relay, a, which, distances))
        pl.when(k == PAIR_AT)(functools.partial(pair_start, f_all, 0))
        ck_copy(k).wait()
        cq_copy(k).wait()
        x_copy(k).wait()
        ct[:kv, span(k)] = ck[span(k), :].T
        grad[...] += jnp.dot(ct[:, span(k)], x[span(k), :], preferred_element_type=F32)

    gradh[...] = grad[...].astype(BF16)
    pair_copy(f_all, 0).wait()
    projected = jnp.dot(
        gradh[...], f_all[...].reshape(gradh.shape[1], f_all.shape[-1]), preferred_element_type=F32
    )
    rank = projected.shape[1] // FS
    part[:, :, :width] = projected.T.reshape(FS, rank, width).astype(BF16)

    @to_plane
    def _(i):
        to = plane(i)
        remote(part.at[to], parts.at[i], sum_sem.at[0], sum_sem.at[1], fs=to).start()

    pair_start(w_all, 1)
    for copy in small[2:]:
        copy.wait()
    seen = parts.at[pl.ds(0, FS - 1)]
    remote(seen, seen, sum_sem.at[0], sum_sem.at[1], fs=partner).wait()
    parts[SELF] = part[me]
    summed = parts[...].astype(F32).sum(axis=0)
    total[...] = summed
    for low, high, first, second in ((0, kv, mk, vk), (kv, width, mq, vq)):
        got = summed[:, low:high]
        first_new = 0.8 * first[...] + 0.2 * got
        second_new = 0.9 * second[...] + 0.1 * got * got
        direction = first_new / (jnp.sqrt(second_new) + 1e-08)
        d_all[me, :, low:high] = direction.astype(BF16)
    mine = d_all.at[me]

    for peer in NEAREST:

        @pl.when(me != peer)
        def _():
            remote(mine, mine, dir_sem.at[0], dir_sem.at[1], fs=peer).start()

    seen = d_all.at[pl.ds(0, FS - 1)]
    remote(seen, seen, dir_sem.at[0], dir_sem.at[1], fs=partner).wait()
    every = d_all[...].astype(F32).reshape(FS * rank, d_all.shape[-1])[:, :width]
    lengths = jnp.sum(every * every, axis=0, keepdims=True)
    lane = lax.broadcasted_iota(jnp.int32, (1, 128), 1)
    squares[tp] = jnp.where(
        lane < 64,
        jnp.sum(lengths[:, :kv], axis=1, keepdims=True),
        jnp.sum(lengths[:, kv:], axis=1, keepdims=True),
    )
    mine = squares.at[tp]
    for d in (2, 1, 3):
        remote(mine, mine, square_sem.at[0], square_sem.at[1], tp=(tp + d) % TP).start()
    factor = f_all[...].reshape(l_steps.shape[0], f_all.shape[-1])
    directions = every.astype(BF16)
    own_steps[...] = jnp.dot(f_all[z, y, c], directions, preferred_element_type=F32)
    l_steps[...] = jnp.dot(factor, directions[:, :kv], preferred_element_type=F32)
    q_steps[...] = lax.dot_general(
        directions[:, kv:], factor, (((0,), (1,)), ((), ())), preferred_element_type=F32
    )
    pair_copy(w_all, 1).wait()
    q_weights[...] = w_all[...].reshape(l_steps.shape[0], w_all.shape[-1])[:, kv:width].T
    seen = squares.at[pl.ds(0, TP - 1)]
    remote(seen, seen, square_sem.at[0], square_sem.at[1], tp=(tp + 1) % TP).wait()


def update_kernel(
    counts,
    w_all, q_weights, l_steps, q_steps, own_steps, squares, total, wq, wk, mq, mk, vq, vk,
    q_new, l_new, q_step, l_step, q_copy, l_copy, q_first, l_first, q_second, l_second,
):
    kv = wk.shape[1]
    width = kv + wq.shape[1]
    sums = squares[0] + squares[1] + squares[2] + squares[3]
    scales = [
        0.5 * jnp.sqrt(jnp.full((1, 1), counts[i], F32)) / jnp.sqrt(sums[:, 64 * i : 64 * i + 1] + 1e-06)
        for i in range(2)
    ]
    summed = total[...]
    for low, high, first, second, first_new, second_new in (
        (0, kv, mk, vk, l_first, l_second),
        (kv, width, mq, vq, q_first, q_second),
    ):
        got = summed[:, low:high]
        first_new[...] = 0.8 * first[...] + 0.2 * got
        second_new[...] = 0.9 * second[...] + 0.1 * got * got
    own = own_steps[...]
    for low, high, scale, weight, new, step in (
        (0, kv, scales[0], wk, l_new, l_step),
        (kv, width, scales[1], wq, q_new, q_step),
    ):
        taken = own[:, low:high] * scale
        step[...] = taken
        new[...] = weight[...] - taken
    weights = w_all[...].reshape(l_steps.shape[0], w_all.shape[-1])
    l_copy[...] = (weights[:, :kv].astype(F32) - l_steps[...] * scales[0]).astype(BF16)
    q_copy[...] = (q_weights[...].astype(F32) - q_steps[...] * scales[1]).astype(BF16)


def body(x, cq, ck, f, wq, wk, mq, mk, vq, vk):
    tokens, model = x.shape
    rows, rank = f.shape
    qw, kv = cq.shape[1], ck.shape[1]
    width = kv + qw
    lanes = -(-width // 128) * 128
    mine = rank // FS
    hbm = pl.BlockSpec(memory_space=pltpu.HBM)
    vmem = pl.BlockSpec(memory_space=pltpu.VMEM)
    shape = jax.ShapeDtypeStruct
    dma = pltpu.SemaphoreType.DMA
    gathered = pl.pallas_call(
        exchange_kernel,
        out_shape=(
            shape((Z, Y, CORES, rows, lanes), BF16),
            shape((qw, FS * rows), BF16),
            shape((FS * rows, kv), F32),
            shape((qw, FS * rows), F32),
            shape((rows, width), F32),
            shape((TP, 1, 128), F32),
            shape((mine, lanes), F32),
        ),
        in_specs=[hbm] * 10,
        out_specs=(vmem,) * 7,
        scratch_shapes=[
            pltpu.VMEM((Z, Y, CORES, rows, rank), BF16),
            pltpu.VMEM((FS, mine, lanes), BF16),
            pltpu.VMEM((tokens, model), BF16),
            pltpu.VMEM((tokens, kv), BF16),
            pltpu.VMEM((width, tokens), BF16),
            pltpu.VMEM((width, model), F32),
            pltpu.VMEM((width, model), BF16),
            pltpu.VMEM((rows, qw), F32),
            pltpu.VMEM((rows, kv), F32),
            pltpu.VMEM((mine, qw), F32),
            pltpu.VMEM((mine, kv), F32),
            pltpu.VMEM((mine, qw), F32),
            pltpu.VMEM((mine, kv), F32),
            pltpu.VMEM((FS, mine, lanes), BF16),
            pltpu.VMEM((FS, mine, lanes), BF16),
            dma((tokens // CHUNK, 3)),
            dma((6,)),
            dma,
            dma((2, 2, 3)),
            dma((2, 2, 3)),
            dma((2, 2)),
            dma((2, 2)),
            dma((2, 2)),
            dma((2,)),
            dma((2,)),
            dma((2,)),
        ],
        compiler_params=pltpu.CompilerParams(
            collective_id=0, has_side_effects=True, vmem_limit_bytes=44 * 1024 * 1024
        ),
        name="exchange",
    )(*(pltpu.with_memory_space_constraint(a, pltpu.HBM) for a in (x, cq.T, ck, f, wq, wk, mq, mk, vq, vk)))
    counts = (rank * kv * TP, rank * qw * TP)
    model_rows = rows * FS
    like = lambda a: shape(a.shape, a.dtype)
    outs = pl.pallas_call(
        functools.partial(update_kernel, counts),
        out_shape=(
            like(wq), like(wk), like(wq), like(wk),
            shape((qw, model_rows), BF16), shape((model_rows, kv), BF16),
            like(mq), like(mk), like(vq), like(vk),
        ),
        in_specs=[vmem] * 13,
        out_specs=(vmem,) * 10,
        compiler_params=pltpu.CompilerParams(vmem_limit_bytes=16 * 1024 * 1024),
        name="update",
    )(*gathered, wq, wk, mq, mk, vq, vk)
    return outs[:4] + (outs[4].T,) + outs[5:]


def solution(mesh):
    return jax.shard_map(
        body,
        mesh=mesh,
        in_specs=(P("fs", None), P("fs", "tp"), P("fs", "tp"), P("fs", None)) + (P("fs", "tp"),) * 6,
        out_specs=(P("fs", "tp"),) * 4 + (P(None, "tp"),) * 2 + (P("fs", "tp"),) * 4,
        check_vma=False,
    )
```

time: 54.4 us -> 35.9 us (0.66)
  local copies, waits for them, and re-layouts: 12.7 us -> 0.03 us
  Pallas kernels: 40.5 us -> 35 us
    unnamed x27 -> x12, local copies, waits for them, and re-layouts: 10.5 us -> 0.03 us
    pallas_call x2, Pallas kernels: 40.5 us -> 35 us  [the longest x1 33.5 us: body(): pl.pallas_call(exchange_kernel, out_shape=(shape((Z, Y, CORES, rows, lane...]
    pallas_call x1 -> x0, local copies, waits for them, and re-layouts: 2.19 us -> none  [body(): pl.pallas_call(functools.partial(update_kernel, counts), out_shape=(lik(w...]
where the time goes in v2:
time: 35.9 us; the launch traced here: 35.8 us
  Pallas kernels  35 us (97%)
  between operations  0.75 us (2%)
    pallas_call x1, Pallas kernels, body(): pl.pallas_call(exchange_kernel, out_shape=(shape((Z, Y, CORES, rows, lane...  33.5 us
    pallas_call x1, Pallas kernels, body(): pl.pallas_call(functools.partial(update_kernel, counts), out_shape=(like(...  1.59 us

profile of v2, /device:TPU:1, one launch (start us, length us, event | category | flops | bytes accessed | tf_op | source)
XLA Modules:
  0.0 35.8 jit_solution(1292586917718410161)
XLA Ops:
  0.6 0.0 copy-start
  0.7 0.0 copy-start.1
  0.7 0.0 copy-start.2
  0.7 0.0 copy-start.3
  0.7 0.0 copy-start.4
  0.7 0.0 copy-start.5
  0.7 33.5 %exchange.1 = (bf16[4,4,2,64,384]{4,3,2,1,0:T(8,128)(2,1)S(1)}, bf16[192,2048]{1,0:T(8,128)(2,1)S(1)}, f32[2048,128]{1,0:T(8,128)S(1)}, f32[192,2048]{1,0:T(8,12...) custom-call(bf16[4608,2048]{1,0:T(8,128)(2,1)} %x_hbm.1, ...), custom_call_target="tpu_custom_call" | custom-call | tf_op jit(solution)/shard_map/exchange/pallas_call | solution.py:261
  34.2 0.0 copy-done
  34.2 0.0 copy-done.1
  34.2 0.0 copy-done.2
  34.2 0.0 copy-done.3
  34.2 0.0 copy-done.4
  34.2 0.0 copy-done.5
  34.2 1.6 %update.1 = (f32[64,192]{1,0:T(8,128)}, f32[64,128]{1,0:T(8,128)}, f32[64,192]{1,0:T(8,128)}, f32[64,128]{1,0:T(8,128)}, bf16[192,2048]{1,0:T(8,128)(2,1)}, /*in...) custom-call(bf16[4,4,2,64,384]{4,3,2,1,0:T(8,128)(2,1)S(1)} %get-tuple-, ...), custom_call_target="tpu_custom_call" | custom-call | tf_op jit(solution)/shard_map/update/pallas_call | solution.py:310
Async XLA Ops:
  0.6 33.5 %copy-start = (f32[64,192]{1,0:T(8,128)S(1)}, f32[64,192]{1,0:T(8,128)}, u32[]{:S(2)}) copy-start(f32[64,192]{1,0:T(8,128)} %wq.1) | copy-start | bytes 147460
  0.7 33.5 %copy-start.1 = (f32[64,128]{1,0:T(8,128)S(1)}, f32[64,128]{1,0:T(8,128)}, u32[]{:S(2)}) copy-start(f32[64,128]{1,0:T(8,128)} %wk.1) | copy-start | bytes 98308
  0.7 33.5 %copy-start.2 = (f32[8,192]{1,0:T(8,128)S(1)}, f32[8,192]{1,0:T(8,128)}, u32[]{:S(2)}) copy-start(f32[8,192]{1,0:T(8,128)} %mq.1) | copy-start | bytes 18436
  0.7 33.5 %copy-start.3 = (f32[8,192]{1,0:T(8,128)S(1)}, f32[8,192]{1,0:T(8,128)}, u32[]{:S(2)}) copy-start(f32[8,192]{1,0:T(8,128)} %vq.1) | copy-start | bytes 18436
  0.7 33.5 %copy-start.4 = (f32[8,128]{1,0:T(8,128)S(1)}, f32[8,128]{1,0:T(8,128)}, u32[]{:S(2)}) copy-start(f32[8,128]{1,0:T(8,128)} %mk.1) | copy-start | bytes 12292
  0.7 33.5 %copy-start.5 = (f32[8,128]{1,0:T(8,128)S(1)}, f32[8,128]{1,0:T(8,128)}, u32[]{:S(2)}) copy-start(f32[8,128]{1,0:T(8,128)} %vk.1) | copy-start | bytes 12292

commit v3 on v2

--- a/solution.py
+++ b/solution.py
@@ -11,10 +11,12 @@
 Z, Y, CORES, TP = 4, 4, 2, 4
 FS = Z * Y * CORES
 BF16, F32 = jnp.bfloat16, jnp.float32
-CHUNK = 768
-NEAR_AT, FAR_AT, W_NEAR_AT, W_FAR_AT, PAIR_AT = 3, 3, 4, 5, 5
-SELF = 20
+CHUNK = 512
+NEAR_AT, FAR_AT, PAIR_AT = 4, 4, 8
 NEAREST = sorted(range(FS), key=lambda i: min(i // 8, 4 - i // 8) + min(i // 2 % 4, 4 - i // 2 % 4))
+
+
+FARTHEST = NEAREST[::-1]
 
 
 def remote(src, dst, send, recv, **where):
@@ -26,7 +28,7 @@
 def exchange_kernel(
     x_hbm, cq_hbm, ck_hbm, f_hbm, wq_hbm, wk_hbm, mq_hbm, mk_hbm, vq_hbm, vk_hbm,
     w_all, q_weights, l_steps, q_steps, own_steps, squares, total,
-    f_all, d_all, x, ck, ct, grad, gradh, wq, wk, mq, mk, vq, vk, part, parts,
+    f_all, d_all, x, ck, ct, grad, wq, wk, mq, mk, vq, vk, part, parts,
     x_sem, small_sem, f_sem, own_send, own_recv, relay_send, relay_recv, pair_sem, sum_sem, dir_sem, square_sem,
 ):
     kv, qw = ck.shape[1], cq_hbm.shape[0]
@@ -36,14 +38,6 @@
     z, y, c = me // (Y * CORES), (me // CORES) % Y, me % CORES
     at = lambda dz, dy, dc: (((z + dz) % Z) * Y + (y + dy) % Y) * CORES + (c + dc) % CORES
     partner = at(0, 0, 1)
-
-    def plane(i):
-        return at((2 + i // (Y * CORES)) % Z, (2 + i // CORES) % Y, i % CORES)
-
-    def to_plane(send):
-        @pl.loop(0, FS)
-        def _(i):
-            pl.when(i != SELF)(functools.partial(send, i))
 
     barrier = pltpu.get_barrier_semaphore()
     axis_peers = [at(0, d, 0) for d in range(1, Y)] + [at(d, 0, 0) for d in range(1, Z)] + [partner]
@@ -142,8 +136,6 @@
         for step, a, which, distances in (
             (NEAR_AT, f_all, 0, (1, 3)),
             (FAR_AT, f_all, 0, (2,)),
-            (W_NEAR_AT, w_all, 1, (1, 3)),
-            (W_FAR_AT, w_all, 1, (2,)),
         ):
             pl.when(k == step)(functools.partial(relay, a, which, distances))
         pl.when(k == PAIR_AT)(functools.partial(pair_start, f_all, 0))
@@ -153,25 +145,25 @@
         ct[:kv, span(k)] = ck[span(k), :].T
         grad[...] += jnp.dot(ct[:, span(k)], x[span(k), :], preferred_element_type=F32)
 
-    gradh[...] = grad[...].astype(BF16)
     pair_copy(f_all, 0).wait()
     projected = jnp.dot(
-        gradh[...], f_all[...].reshape(gradh.shape[1], f_all.shape[-1]), preferred_element_type=F32
+        grad[...].astype(BF16), f_all[...].reshape(grad.shape[1], f_all.shape[-1]), preferred_element_type=F32
     )
     rank = projected.shape[1] // FS
     part[:, :, :width] = projected.T.reshape(FS, rank, width).astype(BF16)
 
-    @to_plane
-    def _(i):
-        to = plane(i)
-        remote(part.at[to], parts.at[i], sum_sem.at[0], sum_sem.at[1], fs=to).start()
-
-    pair_start(w_all, 1)
+    for peer in FARTHEST:
+
+        @pl.when(me != peer)
+        def _():
+            remote(part.at[peer], parts.at[me], sum_sem.at[0], sum_sem.at[1], fs=peer).start()
+
+    relay(w_all, 1, (1, 3, 2))
     for copy in small[2:]:
         copy.wait()
     seen = parts.at[pl.ds(0, FS - 1)]
     remote(seen, seen, sum_sem.at[0], sum_sem.at[1], fs=partner).wait()
-    parts[SELF] = part[me]
+    parts[me] = part[me]
     summed = parts[...].astype(F32).sum(axis=0)
     total[...] = summed
     for low, high, first, second in ((0, kv, mk, vk), (kv, width, mq, vq)):
@@ -188,6 +180,7 @@
         def _():
             remote(mine, mine, dir_sem.at[0], dir_sem.at[1], fs=peer).start()
 
+    pair_start(w_all, 1)
     seen = d_all.at[pl.ds(0, FS - 1)]
     remote(seen, seen, dir_sem.at[0], dir_sem.at[1], fs=partner).wait()
     every = d_all[...].astype(F32).reshape(FS * rank, d_all.shape[-1])[:, :width]
@@ -278,7 +271,6 @@
             pltpu.VMEM((tokens, kv), BF16),
             pltpu.VMEM((width, tokens), BF16),
             pltpu.VMEM((width, model), F32),
-            pltpu.VMEM((width, model), BF16),
             pltpu.VMEM((rows, qw), F32),
             pltpu.VMEM((rows, kv), F32),
             pltpu.VMEM((mine, qw), F32),

time: 35.9 us -> 35.2 us (0.981)
  Pallas kernels: 35 us -> 34.3 us
    pallas_call x1, Pallas kernels: 33.5 us -> 32.7 us  [body(): pl.pallas_call(exchange_kernel, out_shape=(shape((Z, Y, CORES, rows, lane...]
where the time goes in v3:
time: 35.2 us; the launch traced here: 35.1 us
  Pallas kernels  34.3 us (97%)
  between operations  0.75 us (2%)
    pallas_call x1, Pallas kernels, body(): pl.pallas_call(exchange_kernel, out_shape=(shape((Z, Y, CORES, rows, lane...  32.7 us
    pallas_call x1, Pallas kernels, body(): pl.pallas_call(functools.partial(update_kernel, counts), out_shape=(like(...  1.59 us

profile of v3, /device:TPU:1, one launch (start us, length us, event | category | flops | bytes accessed | tf_op | source)
XLA Modules:
  0.0 35.1 jit_solution(7933012594268453759)
XLA Ops:
  0.6 0.0 copy-start
  0.7 0.0 copy-start.1
  0.7 0.0 copy-start.2
  0.7 0.0 copy-start.3
  0.7 0.0 copy-start.4
  0.7 0.0 copy-start.5
  0.7 32.7 %exchange.1 = (bf16[4,4,2,64,384]{4,3,2,1,0:T(8,128)(2,1)S(1)}, bf16[192,2048]{1,0:T(8,128)(2,1)S(1)}, f32[2048,128]{1,0:T(8,128)S(1)}, f32[192,2048]{1,0:T(8,12...) custom-call(bf16[4608,2048]{1,0:T(8,128)(2,1)} %x_hbm.1, ...), custom_call_target="tpu_custom_call" | custom-call | tf_op jit(solution)/shard_map/exchange/pallas_call | solution.py:254
  33.4 0.0 copy-done
  33.4 0.0 copy-done.1
  33.4 0.0 copy-done.2
  33.4 0.0 copy-done.3
  33.4 0.0 copy-done.4
  33.5 0.0 copy-done.5
  33.5 1.6 %update.1 = (f32[64,192]{1,0:T(8,128)}, f32[64,128]{1,0:T(8,128)}, f32[64,192]{1,0:T(8,128)}, f32[64,128]{1,0:T(8,128)}, bf16[192,2048]{1,0:T(8,128)(2,1)}, /*in...) custom-call(bf16[4,4,2,64,384]{4,3,2,1,0:T(8,128)(2,1)S(1)} %get-tuple-, ...), custom_call_target="tpu_custom_call" | custom-call | tf_op jit(solution)/shard_map/update/pallas_call | solution.py:302
Async XLA Ops:
  0.6 32.8 %copy-start = (f32[64,192]{1,0:T(8,128)S(1)}, f32[64,192]{1,0:T(8,128)}, u32[]{:S(2)}) copy-start(f32[64,192]{1,0:T(8,128)} %wq.1) | copy-start | bytes 147460
  0.7 32.8 %copy-start.1 = (f32[64,128]{1,0:T(8,128)S(1)}, f32[64,128]{1,0:T(8,128)}, u32[]{:S(2)}) copy-start(f32[64,128]{1,0:T(8,128)} %wk.1) | copy-start | bytes 98308
  0.7 32.8 %copy-start.2 = (f32[8,192]{1,0:T(8,128)S(1)}, f32[8,192]{1,0:T(8,128)}, u32[]{:S(2)}) copy-start(f32[8,192]{1,0:T(8,128)} %mq.1) | copy-start | bytes 18436
  0.7 32.8 %copy-start.3 = (f32[8,192]{1,0:T(8,128)S(1)}, f32[8,192]{1,0:T(8,128)}, u32[]{:S(2)}) copy-start(f32[8,192]{1,0:T(8,128)} %vq.1) | copy-start | bytes 18436
  0.7 32.8 %copy-start.4 = (f32[8,128]{1,0:T(8,128)S(1)}, f32[8,128]{1,0:T(8,128)}, u32[]{:S(2)}) copy-start(f32[8,128]{1,0:T(8,128)} %mk.1) | copy-start | bytes 12292
  0.7 32.8 %copy-start.5 = (f32[8,128]{1,0:T(8,128)S(1)}, f32[8,128]{1,0:T(8,128)}, u32[]{:S(2)}) copy-start(f32[8,128]{1,0:T(8,128)} %vk.1) | copy-start | bytes 12292

commit v4 on v3

--- a/solution.py
+++ b/solution.py
@@ -28,7 +28,7 @@
 def exchange_kernel(
     x_hbm, cq_hbm, ck_hbm, f_hbm, wq_hbm, wk_hbm, mq_hbm, mk_hbm, vq_hbm, vk_hbm,
     w_all, q_weights, l_steps, q_steps, own_steps, squares, total,
-    f_all, d_all, x, ck, ct, grad, wq, wk, mq, mk, vq, vk, part, parts,
+    f_all, d_all, x, ck, ct, grad, wq, wk, mq, mk, vq, vk, part, parts, crossed, own_square,
     x_sem, small_sem, f_sem, own_send, own_recv, relay_send, relay_recv, pair_sem, sum_sem, dir_sem, square_sem,
 ):
     kv, qw = ck.shape[1], cq_hbm.shape[0]
@@ -121,6 +121,22 @@
         relay_wait(a, which)
         pair_copy(a, which).start()
 
+    def pair_block(a, which, dz, dy):
+        block = a.at[(z + dz) % Z, (y + dy) % Y, c]
+        return remote(block, block, pair_sem.at[which, 0], pair_sem.at[which, 1], fs=partner)
+
+    def pair_early(a, which):
+        for d in range(4):
+            pair_block(a, which, 0, d).start()
+        for d in range(1, 4):
+            pair_block(a, which, d, 0).start()
+
+    def pair_late(a, which):
+        relay_wait(a, which)
+        for dz in range(1, 4):
+            for dy in range(1, 4):
+                pair_block(a, which, dz, dy).start()
+
     own_f.wait()
     pl.semaphore_wait(barrier, len(axis_peers) + TP - 1)
     own_start(f_all, 0)
@@ -138,7 +154,8 @@
             (FAR_AT, f_all, 0, (2,)),
         ):
             pl.when(k == step)(functools.partial(relay, a, which, distances))
-        pl.when(k == PAIR_AT)(functools.partial(pair_start, f_all, 0))
+        pl.when(k == PAIR_AT - 2)(functools.partial(pair_early, f_all, 0))
+        pl.when(k == PAIR_AT)(functools.partial(pair_late, f_all, 0))
         ck_copy(k).wait()
         cq_copy(k).wait()
         x_copy(k).wait()
@@ -180,20 +197,27 @@
         def _():
             remote(mine, mine, dir_sem.at[0], dir_sem.at[1], fs=peer).start()
 
+    lane = lax.broadcasted_iota(jnp.int32, (1, 128), 1)
+
+    def lengths(rows):
+        columns = jnp.sum(rows * rows, axis=0, keepdims=True)
+        return jnp.where(
+            lane < 64,
+            jnp.sum(columns[:, :kv], axis=1, keepdims=True),
+            jnp.sum(columns[:, kv:width], axis=1, keepdims=True),
+        )
+
+    crossed[tp] = jnp.zeros_like(crossed[tp])
+    own_square[...] = lengths(d_all[me].astype(F32))
+    for d in (2, 1, 3):
+        for peer in NEAREST:
+            remote(
+                own_square, crossed.at[tp, me], square_sem.at[0], square_sem.at[1], fs=peer, tp=(tp + d) % TP
+            ).start()
     pair_start(w_all, 1)
     seen = d_all.at[pl.ds(0, FS - 1)]
     remote(seen, seen, dir_sem.at[0], dir_sem.at[1], fs=partner).wait()
     every = d_all[...].astype(F32).reshape(FS * rank, d_all.shape[-1])[:, :width]
-    lengths = jnp.sum(every * every, axis=0, keepdims=True)
-    lane = lax.broadcasted_iota(jnp.int32, (1, 128), 1)
-    squares[tp] = jnp.where(
-        lane < 64,
-        jnp.sum(lengths[:, :kv], axis=1, keepdims=True),
-        jnp.sum(lengths[:, kv:], axis=1, keepdims=True),
-    )
-    mine = squares.at[tp]
-    for d in (2, 1, 3):
-        remote(mine, mine, square_sem.at[0], square_sem.at[1], tp=(tp + d) % TP).start()
     factor = f_all[...].reshape(l_steps.shape[0], f_all.shape[-1])
     directions = every.astype(BF16)
     own_steps[...] = jnp.dot(f_all[z, y, c], directions, preferred_element_type=F32)
@@ -201,10 +225,12 @@
     q_steps[...] = lax.dot_general(
         directions[:, kv:], factor, (((0,), (1,)), ((), ())), preferred_element_type=F32
     )
+    plane_square = lengths(every)
     pair_copy(w_all, 1).wait()
     q_weights[...] = w_all[...].reshape(l_steps.shape[0], w_all.shape[-1])[:, kv:width].T
-    seen = squares.at[pl.ds(0, TP - 1)]
-    remote(seen, seen, square_sem.at[0], square_sem.at[1], tp=(tp + 1) % TP).wait()
+    seen = crossed.at[pl.ds(0, TP - 1)]
+    remote(seen, seen, square_sem.at[0], square_sem.at[1], fs=partner, tp=tp).wait()
+    squares[...] = plane_square + crossed[...].sum(axis=(0, 1))
 
 
 def update_kernel(
@@ -214,7 +240,7 @@
 ):
     kv = wk.shape[1]
     width = kv + wq.shape[1]
-    sums = squares[0] + squares[1] + squares[2] + squares[3]
+    sums = squares[...]
     scales = [
         0.5 * jnp.sqrt(jnp.full((1, 1), counts[i], F32)) / jnp.sqrt(sums[:, 64 * i : 64 * i + 1] + 1e-06)
         for i in range(2)
@@ -259,7 +285,7 @@
             shape((FS * rows, kv), F32),
             shape((qw, FS * rows), F32),
             shape((rows, width), F32),
-            shape((TP, 1, 128), F32),
+            shape((1, 128), F32),
             shape((mine, lanes), F32),
         ),
         in_specs=[hbm] * 10,
@@ -279,6 +305,8 @@
             pltpu.VMEM((mine, kv), F32),
             pltpu.VMEM((FS, mine, lanes), BF16),
             pltpu.VMEM((FS, mine, lanes), BF16),
+            pltpu.VMEM((TP, FS, 1, 128), F32),
+            pltpu.VMEM((1, 128), F32),
             dma((tokens // CHUNK, 3)),
             dma((6,)),
             dma,

time: 35.2 us -> 34.7 us (0.986)
  Pallas kernels: 34.3 us -> 33.8 us
    pallas_call x1, Pallas kernels: 32.7 us -> 32.2 us  [body(): pl.pallas_call(exchange_kernel, out_shape=(shape((Z, Y, CORES, rows, lane...]
where the time goes in v4:
time: 34.7 us; the launch traced here: 34.6 us
  Pallas kernels  33.8 us (97%)
  between operations  0.75 us (2%)
    pallas_call x1, Pallas kernels, body(): pl.pallas_call(exchange_kernel, out_shape=(shape((Z, Y, CORES, rows, lane...  32.2 us
    pallas_call x1, Pallas kernels, body(): pl.pallas_call(functools.partial(update_kernel, counts), out_shape=(like(...  1.58 us

profile of v4, /device:TPU:1, one launch (start us, length us, event | category | flops | bytes accessed | tf_op | source)
XLA Modules:
  0.0 34.6 jit_solution(6928610308613955771)
XLA Ops:
  0.6 0.0 copy-start
  0.7 0.0 copy-start.1
  0.7 0.0 copy-start.2
  0.7 0.0 copy-start.3
  0.7 0.0 copy-start.4
  0.7 0.0 copy-start.5
  0.7 32.2 %exchange.1 = (bf16[4,4,2,64,384]{4,3,2,1,0:T(8,128)(2,1)S(1)}, bf16[192,2048]{1,0:T(8,128)(2,1)S(1)}, f32[2048,128]{1,0:T(8,128)S(1)}, f32[192,2048]{1,0:T(8,12...) custom-call(bf16[4608,2048]{1,0:T(8,128)(2,1)} %x_hbm.1, bf16[192,4608]{1,0:T(8,128)(2,1)} %bitcast.2, ...), custom_call_target="tpu_custom_call" | custom-call | tf_op jit(solution)/shard_map/exchange/pallas_call | solution.py:280
  32.9 0.0 copy-done
  33.0 0.0 copy-done.1
  33.0 0.0 copy-done.2
  33.0 0.0 copy-done.3
  33.0 0.0 copy-done.4
  33.0 0.0 copy-done.5
  33.0 1.6 %update.1 = (f32[64,192]{1,0:T(8,128)}, f32[64,128]{1,0:T(8,128)}, f32[64,192]{1,0:T(8,128)}, f32[64,128]{1,0:T(8,128)}, bf16[192,2048]{1,0:T(8,128)(2,1)}, /*in...) custom-call(bf16[4,4,2,64,384]{4,3,2,1,0:T(8,128)(2,1)S(1)} %get-tuple-, ...), custom_call_target="tpu_custom_call" | custom-call | tf_op jit(solution)/shard_map/update/pallas_call | solution.py:330
Async XLA Ops:
  0.6 32.3 %copy-start = (f32[64,192]{1,0:T(8,128)S(1)}, f32[64,192]{1,0:T(8,128)}, u32[]{:S(2)}) copy-start(f32[64,192]{1,0:T(8,128)} %wq.1) | copy-start | bytes 147460
  0.7 32.3 %copy-start.1 = (f32[64,128]{1,0:T(8,128)S(1)}, f32[64,128]{1,0:T(8,128)}, u32[]{:S(2)}) copy-start(f32[64,128]{1,0:T(8,128)} %wk.1) | copy-start | bytes 98308
  0.7 32.3 %copy-start.2 = (f32[8,192]{1,0:T(8,128)S(1)}, f32[8,192]{1,0:T(8,128)}, u32[]{:S(2)}) copy-start(f32[8,192]{1,0:T(8,128)} %mq.1) | copy-start | bytes 18436
  0.7 32.3 %copy-start.3 = (f32[8,192]{1,0:T(8,128)S(1)}, f32[8,192]{1,0:T(8,128)}, u32[]{:S(2)}) copy-start(f32[8,192]{1,0:T(8,128)} %vq.1) | copy-start | bytes 18436
  0.7 32.3 %copy-start.4 = (f32[8,128]{1,0:T(8,128)S(1)}, f32[8,128]{1,0:T(8,128)}, u32[]{:S(2)}) copy-start(f32[8,128]{1,0:T(8,128)} %mk.1) | copy-start | bytes 12292
  0.7 32.3 %copy-start.5 = (f32[8,128]{1,0:T(8,128)S(1)}, f32[8,128]{1,0:T(8,128)}, u32[]{:S(2)}) copy-start(f32[8,128]{1,0:T(8,128)} %vk.1) | copy-start | bytes 12292
